TPU v7x, 32 devices: a whole 2x2x4 slice. The times are simulated.
32 devices in a mesh: st: 4 (over y, x), tp: 8 (over z, core).
Axes of the slice: x: 2, y: 2, z: 4, core: 2. Of those that a mesh axis runs over, the one named last changes fastest.
Arguments:
- tokens: bfloat16 [2048, 4096], P('st', 'tp'), may hold values from -6 to 6
- w_query: bfloat16 [4096, 2048], P(None, 'tp'), may hold values from -0.09375 to 0.09375
- w_key: bfloat16 [4096, 2048], P(None, 'tp'), may hold values from -0.09375 to 0.09375
- w_value: bfloat16 [4096, 4096], P(None, 'tp'), may hold values from -0.09375 to 0.09375
- w_mem_query: bfloat16 [4096, 2048], P(None, 'tp'), may hold values from -0.09375 to 0.09375
- w_mem_key: bfloat16 [4096, 2048], P(None, 'tp'), may hold values from -0.09375 to 0.09375
- w_mem_value: bfloat16 [4096, 2048], P(None, 'tp'), may hold values from -0.09375 to 0.09375
- w_gate: bfloat16 [4096, 16], P(None, 'tp'), may hold values from -0.09375 to 0.09375
- w_lift: bfloat16 [16, 128, 256], P('tp'), may hold values from -4 to 4
- decay_rate: float32 [16], P('tp'), may hold values from 0.000390625 to 0.1
- store: bfloat16 [512, 64, 4096], P('st', None, 'tp'), may hold values from -6 to 6
- passage_ids: int32 [16, 2], P('st'), may hold values from 0 to 511, as said below
Outputs:
- mixed: bfloat16 [2048, 4096], P('st', 'tp')
Inputs may be any that keep to these rules, and one draw needn't show every extreme that they name: `passage_ids`: passage p is held by index p // 128 of st. Among the requests of the rows of one device along st, at most 4 name passages held by one index of st, and in every draw some index receives exactly 4 of them.
All inputs are finite; a program needn't handle non-finite values.
Results may differ from a plain program's by a relative error of at most 0.0095.
Values may be sent and summed in bfloat16 or wider, within the bound.
A program may use at most 64 MiB of HBM per device.

v0:
```python
import functools

import jax
import jax.numpy as jnp
import numpy as np
from jax import lax
from jax.experimental import pallas as pl
from jax.experimental.pallas import tpu as pltpu
from jax.sharding import PartitionSpec as P

KEY_DIM = 128
VALUE_DIM = 256
MEM_DIM = 128
SEQ_LEN = 512
NORM_EPS = 1e-06
ROPE_BASE = 10000.0
CORES = 2
CHUNK = 128
MESH = pl.DeviceIdType.MESH
F32 = jnp.float32
BF16 = jnp.bfloat16


def dot(a, b):
    return jnp.dot(a, b, preferred_element_type=F32)


def dot_nt(a, b):
    return lax.dot_general(a, b, (((1,), (1,)), ((), ())), preferred_element_type=F32)


def kernel(
    n_st, n_tp, cap, picks, held,
    rate_ref, tok_hbm, wq_hbm, wk_hbm, wv_hbm, wm_hbm, wmk_hbm, wmv_hbm, wg_ref, lift_ref,
    cos_ref, sin_ref, store_hbm, ids_hbm,
    out_ref,
    tok, rows, wq, wk, wv, wm, wmk, wmv, store, slots, landed, ids_v, ids_s,
    acc_q, acc_k, acc_v, acc_m, acc_g, acc_s, acc_mk, acc_mv,
    rq, rk, rv, mq, ret, gate,
    load_sem, id_send, id_recv, pass_send, pass_recv,
    t_recv, t_send, t_left, t_pair, r_recv, r_send, r_left, r_pair,
):
    st = lax.axis_index("st")
    me = lax.axis_index("tp")
    z = me // CORES
    core = me % CORES
    n_z = n_tp // CORES
    total, cols = tok.shape[1:]
    heads = mq.shape[1] // MEM_DIM
    requests = ids_s.shape[2]
    pass_rows = store.shape[1]

    loads = []
    pairs = [(store_hbm, store), (ids_hbm, ids_v.at[st]), (tok_hbm, tok.at[me]), (wq_hbm, wq), (wk_hbm, wk),
             (wv_hbm, wv), (wm_hbm, wm), (wmk_hbm, wmk), (wmv_hbm, wmv)]
    for i, (src, dst) in enumerate(pairs):
        loads.append(pltpu.make_async_copy(src, dst, load_sem.at[i]))
        loads[-1].start()

    barrier = pltpu.get_barrier_semaphore()
    has_right = z < n_z - 1
    has_left = z > 0

    @pl.when(has_right)
    def _():
        pl.semaphore_signal(barrier, inc=1, device_id=(st, me + CORES), device_id_type=MESH)

    @pl.when(has_left)
    def _():
        pl.semaphore_signal(barrier, inc=1, device_id=(st, me - CORES), device_id_type=MESH)

    pair = z * CORES + (1 - core)
    pl.semaphore_signal(barrier, inc=1, device_id=(st, pair), device_id_type=MESH)
    for d in range(1, n_st):
        pl.semaphore_signal(barrier, inc=1, device_id=((st + d) % n_st, me), device_id_type=MESH)
    pl.semaphore_wait(barrier, n_st + has_right.astype(jnp.int32) + has_left.astype(jnp.int32))

    def remote(src, dst, send, recv, to_st, to_tp):
        return pltpu.make_async_remote_copy(
            src_ref=src, dst_ref=dst, send_sem=send, recv_sem=recv,
            device_id=(to_st, to_tp), device_id_type=MESH)

    def line(buf, sems):
        recv, send, left, pairing = sems

        def right_copy(j, src=None):
            return remote(buf.at[j] if src is None else src, buf.at[j], send.at[j], recv.at[j], st, me + CORES)

        def left_copy(j, src=None):
            sem = left.at[0] if src is not None else send.at[j]
            return remote(buf.at[j] if src is None else src, buf.at[j], sem, recv.at[j], st, me - CORES)

        def pair_copy(j, src=None):
            return remote(buf.at[j] if src is None else src, buf.at[j], pairing.at[j], recv.at[j], st, pair)

        def send_own(src):
            @pl.when(has_right)
            def _():
                right_copy(me, src).start()

            @pl.when(has_left)
            def _():
                left_copy(me, src).start()
            pair_copy(me, src).start()

        def relay(d):
            from_left = me - CORES * d
            from_right = me + CORES * d

            @pl.when(from_left >= 0)
            def _():
                pair_copy(from_left).wait_recv()

                @pl.when(has_right)
                def _():
                    right_copy(from_left).start()
                pair_copy(from_left).start()

            @pl.when(from_right < n_tp)
            def _():
                pair_copy(from_right).wait_recv()

                @pl.when(has_left)
                def _():
                    left_copy(from_right).start()
                pair_copy(from_right).start()

        def drain(src):
            @pl.when(has_right)
            def _():
                right_copy(me, src).wait_send()

            @pl.when(has_left)
            def _():
                left_copy(me, src).wait_send()
            pair_copy(me, src).wait_send()

            def step(d, carry):
                from_left = me - CORES * d
                from_right = me + CORES * d

                @pl.when(from_left >= 0)
                def _():
                    @pl.when(has_right)
                    def _():
                        right_copy(from_left).wait_send()
                    pair_copy(from_left).wait_send()

                @pl.when(from_right < n_tp)
                def _():
                    @pl.when(has_left)
                    def _():
                        left_copy(from_right).wait_send()
                    pair_copy(from_right).wait_send()
                return carry
            lax.fori_loop(1, n_z, step, 0)

        def consume(low, high, take):
            def step(q, carry):
                d, side, which = q // 4, (q // 2) % 2, q % 2
                at = z + (2 * side - 1) * d
                j = at * CORES + which
                valid = (at >= 0) & (at < n_z) & ((d > 0) | (side == 0))

                @pl.when(valid)
                def _():
                    @pl.when(which != core)
                    def _():
                        pair_copy(j).wait_recv()
                    take(j)
                return carry
            lax.fori_loop(4 * low, 4 * high, step, 0)

        return send_own, relay, drain, consume

    tok_send, tok_relay, tok_drain, tok_consume = line(tok, (t_recv, t_send, t_left, t_pair))
    row_send, row_relay, row_drain, row_consume = line(rows, (r_recv, r_send, r_left, r_pair))

    def id_copy(d):
        return remote(ids_hbm, ids_v.at[st], id_send.at[d], id_recv.at[st], (st + d) % n_st, me)

    def id_wait(d):
        other = (st + d) % n_st
        return remote(ids_hbm, ids_v.at[other], id_send.at[d], id_recv.at[other], other, me)

    for d in range(1, n_st):
        id_copy(d).start()
    tok_send(tok_hbm)

    for ref in (acc_q, acc_k, acc_v, acc_m, acc_g, acc_s, acc_mk, acc_mv):
        ref[...] = jnp.zeros_like(ref)

    loads[1].wait()
    for d in range(1, n_st):
        id_wait(d).wait_recv()
    to_scalar = pltpu.make_async_copy(ids_v, ids_s, load_sem.at[len(pairs)])
    to_scalar.start()
    to_scalar.wait()
    loads[0].wait()

    def asked(source, k):
        found = jnp.int32(0)
        seen = jnp.int32(0)
        for i in range(requests):
            ident = ids_s[source, 0, i]
            mine = (ident // held) == st
            found = jnp.where(mine & (seen == k), ident % held, found)
            seen = seen + mine.astype(jnp.int32)
        return found

    def fill(d, carry):
        source = (st + d) % n_st
        for k in range(cap):
            slots[d, k] = store[asked(source, k)]
        return carry
    lax.fori_loop(1, n_st, fill, 0)

    def pass_copy(d):
        return remote(slots.at[d], landed.at[st], pass_send.at[d], pass_recv.at[st], (st + d) % n_st, me)

    def pass_wait(d):
        other = (st + d) % n_st
        return remote(slots.at[d], landed.at[other], pass_send.at[d], pass_recv.at[other], other, me)

    for d in range(1, n_st):
        pass_copy(d).start()
    for k in range(cap):
        landed[st, k] = store[asked(st, k)]

    tok_relay(1)

    for d in range(1, n_st):
        pass_wait(d).wait_recv()
    for i in range(requests):
        ident = ids_s[st, 0, i]
        owner = ident // held
        order = jnp.int32(0)
        for e in range(i):
            order = order + ((ids_s[st, 0, e] // held) == owner).astype(jnp.int32)
        rows[me, pl.ds(i * pass_rows, pass_rows), :] = landed[owner, jnp.minimum(order, cap - 1)]
    row_send(None)

    for i in range(2, 9):
        loads[i].wait()

    def take_tokens(j):
        at = pl.ds(pl.multiple_of(j * cols, cols), cols)

        def part(c, carry):
            here = pl.ds(pl.multiple_of(c * 256, 256), 256)
            x = tok[j, here, :]
            acc_q[here, :] += dot(x, wq[at, :])
            acc_k[here, :] += dot(x, wk[at, :])
            acc_v[here, :] += dot(x, wv[at, :])
            acc_m[here, :] += dot(x, wm[at, :])
            wide = x.astype(F32)
            if heads > 1:
                acc_g[here, :] += dot_nt(x, wg_ref[:, at])
            else:
                acc_g[here, :] += jnp.sum(wide * wg_ref[:, at].astype(F32), axis=1, keepdims=True)
            squares = acc_s[here, :]
            for piece in range(cols // 128):
                slab = wide[:, piece * 128:(piece + 1) * 128]
                squares = squares + slab * slab
            acc_s[here, :] = squares
            return carry
        lax.fori_loop(0, total // 256, part, 0)

    tok_consume(0, 2, take_tokens)

    def token_stage(d, carry):
        tok_relay(d)
        tok_consume(d, d + 1, take_tokens)
        return carry
    lax.fori_loop(2, n_z, token_stage, 0)

    row_relay(1)

    def prepare(c, carry):
        here = pl.ds(pl.multiple_of(c * CHUNK, CHUNK), CHUNK)
        scale = lax.rsqrt(jnp.sum(acc_s[here, :], axis=1, keepdims=True) / (n_tp * cols) + NORM_EPS)
        cosine, sine = cos_ref[here, :], sin_ref[here, :]

        def rotate(v):
            return v * cosine + pltpu.roll(v, KEY_DIM // 2, 1) * sine
        for h in range(heads):
            at = slice(h * KEY_DIM, (h + 1) * KEY_DIM)
            rq[here, at] = rotate(acc_q[here, at] * scale).astype(BF16)
            rk[here, at] = (rotate(acc_k[here, at] * scale) * KEY_DIM ** (-0.5)).astype(BF16)
            m = acc_m[here, at]
            mq[here, at] = (m * lax.rsqrt(jnp.mean(m * m, axis=1, keepdims=True) + NORM_EPS)).astype(BF16)
        rv[here, :] = (acc_v[here, :] * scale).astype(BF16)
        gate[here, :] = jax.nn.sigmoid(acc_g[here, :] * scale)
        return carry
    lax.fori_loop(0, total // CHUNK, prepare, 0)

    def retain(c, carry):
        here = pl.ds(pl.multiple_of(c * CHUNK, CHUNK), CHUNK)
        start = (c * CHUNK) // SEQ_LEN * SEQ_LEN
        whole = pl.ds(pl.multiple_of(start, SEQ_LEN), SEQ_LEN)
        t = lax.broadcasted_iota(jnp.int32, (CHUNK, SEQ_LEN), 0) + (c * CHUNK - start)
        s = lax.broadcasted_iota(jnp.int32, (CHUNK, SEQ_LEN), 1)
        gap = (t - s).astype(F32)
        for h in range(heads):
            at = slice(h * KEY_DIM, (h + 1) * KEY_DIM)
            wide = slice(h * VALUE_DIM, (h + 1) * VALUE_DIM)
            decay = jnp.where(gap >= 0.0, jnp.exp(-rate_ref[h] * jnp.maximum(gap, 0.0)), 0.0)
            scores = dot_nt(rq[here, at], rk[whole, at]) * decay
            upper = scores.astype(BF16)
            lower = (scores - upper.astype(F32)).astype(BF16)
            value = rv[whole, wide]
            o = dot(upper, value) + dot(lower, value)
            o = o - jnp.mean(o, axis=1, keepdims=True)
            ret[here, wide] = o * lax.rsqrt(jnp.mean(o * o, axis=1, keepdims=True) + NORM_EPS)
        return carry
    lax.fori_loop(0, total // CHUNK, retain, 0)

    def take_rows(j):
        at = pl.ds(pl.multiple_of(j * cols, cols), cols)

        def part(c, carry):
            here = pl.ds(pl.multiple_of(c * 256, 256), 256)
            x = rows[j, here, :]
            acc_mk[here, :] += dot(x, wmk[at, :])
            acc_mv[here, :] += dot(x, wmv[at, :])
            return carry
        lax.fori_loop(0, rows.shape[1] // 256, part, 0)

    row_consume(0, 2, take_rows)

    def row_stage(d, carry):
        row_relay(d)
        row_consume(d, d + 1, take_rows)
        return carry
    lax.fori_loop(2, n_z, row_stage, 0)

    blocks = requests // picks
    block = total // blocks
    keys = picks * pass_rows

    def attend(b, carry):
        here = pl.ds(pl.multiple_of(b * block, block), block)
        there = pl.ds(pl.multiple_of(b * keys, keys), keys)
        for h in range(heads):
            at = slice(h * MEM_DIM, (h + 1) * MEM_DIM)
            wide = slice(h * VALUE_DIM, (h + 1) * VALUE_DIM)
            k = acc_mk[there, at]
            k = (k * lax.rsqrt(jnp.mean(k * k, axis=1, keepdims=True) + NORM_EPS)).astype(BF16)
            v = acc_mv[there, at].astype(BF16)
            exponent = jnp.exp(dot_nt(mq[here, at], k) * MEM_DIM ** (-0.5))
            mass = jnp.sum(exponent, axis=1, keepdims=True)
            o = (dot(exponent.astype(BF16), v) / mass).astype(BF16)
            lifted = dot(o, lift_ref[h])
            out_ref[here, wide] = (ret[here, wide] + gate[here, h:h + 1] * lifted).astype(BF16)
        return carry
    lax.fori_loop(0, blocks, attend, 0)

    for d in range(1, n_st):
        id_copy(d).wait_send()
        pass_copy(d).wait_send()
    tok_drain(tok_hbm)
    row_drain(None)


def rotary_tables(total):
    half = KEY_DIM // 2
    angle = (np.arange(total) % SEQ_LEN)[:, None] * ROPE_BASE ** (-np.arange(half) / half)[None, :]
    cosine, sine = np.cos(angle), np.sin(angle)
    return (np.concatenate([cosine, cosine], 1).astype(np.float32),
            np.concatenate([-sine, sine], 1).astype(np.float32))


def solution(mesh):
    n_st, n_tp = mesh.shape["st"], mesh.shape["tp"]

    def per_device(tokens, w_query, w_key, w_value, w_mem_query, w_mem_key, w_mem_value, w_gate, w_lift,
                   decay_rate, store, passage_ids):
        total, cols = tokens.shape
        heads = decay_rate.shape[0]
        blocks, picks = passage_ids.shape
        requests = blocks * picks
        held, pass_rows, _ = store.shape
        cap = max(1, 2 * requests // n_st)
        cosine, sine = rotary_tables(total)
        hbm = pl.BlockSpec(memory_space=pl.ANY)
        vmem = pl.BlockSpec(memory_space=pltpu.VMEM)
        smem = pl.BlockSpec(memory_space=pltpu.SMEM)
        V = pltpu.VMEM
        dma = pltpu.SemaphoreType.DMA
        wide = w_value.shape[1]
        key_cols, mem_cols = w_query.shape[1], w_mem_query.shape[1]
        scratch = [
            V((n_tp, total, cols), BF16), V((n_tp, requests * pass_rows, cols), BF16),
            V(w_query.shape, BF16), V(w_key.shape, BF16), V(w_value.shape, BF16),
            V(w_mem_query.shape, BF16), V(w_mem_key.shape, BF16), V(w_mem_value.shape, BF16),
            V(store.shape, BF16), V((n_st, cap, pass_rows, cols), BF16), V((n_st, cap, pass_rows, cols), BF16),
            V((n_st, 1, requests), jnp.int32), pltpu.SMEM((n_st, 1, requests), jnp.int32),
            V((total, key_cols), F32), V((total, key_cols), F32), V((total, wide), F32), V((total, mem_cols), F32),
            V((total, heads), F32), V((total, 128), F32),
            V((requests * pass_rows, mem_cols), F32), V((requests * pass_rows, mem_cols), F32),
            V((total, key_cols), BF16), V((total, key_cols), BF16), V((total, wide), BF16), V((total, mem_cols), BF16),
            V((total, wide), F32), V((total, heads), F32),
            dma((10,)), dma((n_st,)), dma((n_st,)), dma((n_st,)), dma((n_st,)),
            dma((n_tp,)), dma((n_tp,)), dma((1,)), dma((n_tp,)),
            dma((n_tp,)), dma((n_tp,)), dma((1,)), dma((n_tp,)),
        ]
        return pl.pallas_call(
            functools.partial(kernel, n_st, n_tp, cap, picks, held),
            out_shape=jax.ShapeDtypeStruct((total, heads * VALUE_DIM), BF16),
            in_specs=[smem] + [hbm] * 7 + [vmem] * 4 + [hbm] * 2,
            out_specs=vmem,
            scratch_shapes=scratch,
            compiler_params=pltpu.CompilerParams(
                collective_id=0, has_side_effects=True, vmem_limit_bytes=60 * 1024 * 1024),
        )(decay_rate, tokens, w_query, w_key, w_value, w_mem_query, w_mem_key, w_mem_value,
          w_gate.T, w_lift, jnp.asarray(cosine), jnp.asarray(sine), store, passage_ids.reshape(1, requests))

    in_specs = (P("st", "tp"),) + (P(None, "tp"),) * 7 + (
        P("tp", None, None), P("tp"), P("st", None, "tp"), P("st", None))
    return jax.shard_map(per_device, mesh=mesh, in_specs=in_specs, out_specs=P("st", "tp"), check_vma=False)
```

profile of v0, /device:TPU:1, one launch (start us, length us, event | category | flops | bytes accessed | tf_op | source)
XLA Modules:
  0.0 86.9 jit_solution(2320955743119399149)
XLA Ops:
  0.0 0.8 copy.16
  0.8 0.6 reshape.3.ids_hbm
  1.4 83.7 %shard_map.136 = bf16[512,512]{1,0:T(8,128)(2,1)} custom-call(f32[2]{0:T(128)} %rate_ref.1, bf16[512,512]{1,0:T(8,128)(2,1)} %tok_hbm.1, bf16[4096,256]{1,0:T(8,128)(2,1)} %wq_hbm.1, bf16[4096,256]{1,0:T(8,128)(2,1)} %wk_hbm.1, bf16[4096,512]{1,0:T(8,128)(2,1)} %wv_hbm.1, bf16[4096,256]{1,0:T(8,128)(2,1)} %wm_hbm.1, bf16[4096,256]{1,0:T(8,128)(2,1)} %wmk_hbm.1, ...), custom_call_target="tpu_custom_call" | custom-call | tf_op jit(solution)/shard_map/pallas_call | solution.py:407
  85.1 1.9 %copy.18 = bf16[512,512]{1,0:T(8,128)(2,1)} copy(bf16[512,512]{1,0:T(8,128)(2,1)} %shard_map.136) | data formatting | bytes 1048576
where the time goes:
time: 87.1 us; the launch traced here: 86.9 us
  Pallas kernels  83.7 us (96%)
  local copies, waits for them, and re-layouts  3.23 us (4%)
    pallas_call x1, Pallas kernels, per_device(): pl.pallas_call(functools.partial(kernel, n_st, n_tp, cap, picks, held), o...  83.7 us
    unnamed x2, local copies, waits for them, and re-layouts  2.63 us

commit v1 on v0

--- a/solution.py
+++ b/solution.py
@@ -16,6 +16,8 @@
 ROPE_BASE = 10000.0
 CORES = 2
 CHUNK = 128
+PIECES = 2
+SPLIT = 1
 MESH = pl.DeviceIdType.MESH
 F32 = jnp.float32
 BF16 = jnp.bfloat16
@@ -31,10 +33,10 @@
 
 def kernel(
     n_st, n_tp, cap, picks, held,
-    rate_ref, tok_hbm, wq_hbm, wk_hbm, wv_hbm, wm_hbm, wmk_hbm, wmv_hbm, wg_ref, lift_ref,
-    cos_ref, sin_ref, store_hbm, ids_hbm,
+    rate_ref, tok_hbm, wq_hbm, wk_hbm, wv_hbm, wm_hbm, wmk_hbm, wmv_hbm, wg_ref, lift_hbm,
+    cos_hbm, sin_hbm, store_hbm, ids_hbm,
     out_ref,
-    tok, rows, wq, wk, wv, wm, wmk, wmv, store, slots, landed, ids_v, ids_s,
+    tok, rows, cos_ref, sin_ref, lift_ref, wq, wk, wv, wm, wmk, wmv, store, slots, landed, ids_v, ids_s,
     acc_q, acc_k, acc_v, acc_m, acc_g, acc_s, acc_mk, acc_mv,
     rq, rk, rv, mq, ret, gate,
     load_sem, id_send, id_recv, pass_send, pass_recv,
@@ -47,15 +49,16 @@
     n_z = n_tp // CORES
     total, cols = tok.shape[1:]
     heads = mq.shape[1] // MEM_DIM
-    requests = ids_s.shape[2]
+    requests = ids_s.shape[1] * ids_s.shape[2]
     pass_rows = store.shape[1]
 
     loads = []
     pairs = [(store_hbm, store), (ids_hbm, ids_v.at[st]), (tok_hbm, tok.at[me]), (wq_hbm, wq), (wk_hbm, wk),
-             (wv_hbm, wv), (wm_hbm, wm), (wmk_hbm, wmk), (wmv_hbm, wmv)]
+             (wv_hbm, wv), (wm_hbm, wm), (wmk_hbm, wmk), (wmv_hbm, wmv),
+             (cos_hbm, cos_ref), (sin_hbm, sin_ref), (lift_hbm, lift_ref)]
     for i, (src, dst) in enumerate(pairs):
         loads.append(pltpu.make_async_copy(src, dst, load_sem.at[i]))
-        loads[-1].start()
+    loads[1].start()
 
     barrier = pltpu.get_barrier_semaphore()
     has_right = z < n_z - 1
@@ -82,60 +85,64 @@
 
     def line(buf, sems):
         recv, send, left, pairing = sems
-
-        def right_copy(j, src=None):
-            return remote(buf.at[j] if src is None else src, buf.at[j], send.at[j], recv.at[j], st, me + CORES)
-
-        def left_copy(j, src=None):
-            sem = left.at[0] if src is not None else send.at[j]
-            return remote(buf.at[j] if src is None else src, buf.at[j], sem, recv.at[j], st, me - CORES)
-
-        def pair_copy(j, src=None):
-            return remote(buf.at[j] if src is None else src, buf.at[j], pairing.at[j], recv.at[j], st, pair)
+        size = buf.shape[1] // PIECES
+
+        def piece(j, p):
+            return buf.at[j, pl.ds(p * size, size)]
+
+        def own_piece(src, p):
+            return piece(me, p) if src is None else src.at[pl.ds(p * size, size)]
+
+        def right_copy(j, p, src=None):
+            return remote(piece(j, p) if src is None else src, piece(j, p), send.at[j, p], recv.at[j, p],
+                          st, me + CORES)
+
+        def left_copy(j, p, src=None):
+            sem = left.at[0, p] if src is not None else send.at[j, p]
+            return remote(piece(j, p) if src is None else src, piece(j, p), sem, recv.at[j, p], st, me - CORES)
+
+        def pair_copy(j, p, src=None):
+            return remote(piece(j, p) if src is None else src, piece(j, p), pairing.at[j, p], recv.at[j, p], st, pair)
 
         def send_own(src):
-            @pl.when(has_right)
-            def _():
-                right_copy(me, src).start()
-
-            @pl.when(has_left)
-            def _():
-                left_copy(me, src).start()
-            pair_copy(me, src).start()
-
-        def relay(d):
+            for p in range(PIECES):
+                own = own_piece(src, p)
+
+                @pl.when(has_right)
+                def _():
+                    right_copy(me, p, own).start()
+
+                @pl.when(has_left)
+                def _():
+                    left_copy(me, p, own).start()
+            for p in range(PIECES):
+                pair_copy(me, p, own_piece(src, p)).start()
+
+        def relay(d, p):
             from_left = me - CORES * d
             from_right = me + CORES * d
 
             @pl.when(from_left >= 0)
             def _():
-                pair_copy(from_left).wait_recv()
+                pair_copy(from_left, p).wait_recv()
 
                 @pl.when(has_right)
                 def _():
-                    right_copy(from_left).start()
-                pair_copy(from_left).start()
+                    right_copy(from_left, p).start()
+                pair_copy(from_left, p).start()
 
             @pl.when(from_right < n_tp)
             def _():
-                pair_copy(from_right).wait_recv()
+                pair_copy(from_right, p).wait_recv()
 
                 @pl.when(has_left)
                 def _():
-                    left_copy(from_right).start()
-                pair_copy(from_right).start()
+                    left_copy(from_right, p).start()
+                pair_copy(from_right, p).start()
 
         def drain(src):
-            @pl.when(has_right)
-            def _():
-                right_copy(me, src).wait_send()
-
-            @pl.when(has_left)
-            def _():
-                left_copy(me, src).wait_send()
-            pair_copy(me, src).wait_send()
-
-            def step(d, carry):
+            def step(q, carry):
+                d, p = q // PIECES, q % PIECES
                 from_left = me - CORES * d
                 from_right = me + CORES * d
 
@@ -143,19 +150,23 @@
                 def _():
                     @pl.when(has_right)
                     def _():
-                        right_copy(from_left).wait_send()
-                    pair_copy(from_left).wait_send()
-
-                @pl.when(from_right < n_tp)
+                        right_copy(from_left, p).wait_send()
+                    pair_copy(from_left, p).wait_send()
+
+                @pl.when((d > 0) & (from_right < n_tp))
                 def _():
                     @pl.when(has_left)
                     def _():
-                        left_copy(from_right).wait_send()
-                    pair_copy(from_right).wait_send()
+                        left_copy(from_right, p).wait_send()
+                    pair_copy(from_right, p).wait_send()
                 return carry
-            lax.fori_loop(1, n_z, step, 0)
-
-        def consume(low, high, take):
+            for p in range(PIECES):
+                @pl.when(has_left)
+                def _():
+                    left_copy(me, p, own_piece(src, p)).wait_send()
+            lax.fori_loop(0, PIECES * n_z, step, 0)
+
+        def consume(low, high, take, p):
             def step(q, carry):
                 d, side, which = q // 4, (q // 2) % 2, q % 2
                 at = z + (2 * side - 1) * d
@@ -166,8 +177,8 @@
                 def _():
                     @pl.when(which != core)
                     def _():
-                        pair_copy(j).wait_recv()
-                    take(j)
+                        pair_copy(j, p).wait_recv()
+                    take(j, p)
                 return carry
             lax.fori_loop(4 * low, 4 * high, step, 0)
 
@@ -186,6 +197,8 @@
     for d in range(1, n_st):
         id_copy(d).start()
     tok_send(tok_hbm)
+    loads[0].start()
+    loads[2].start()
 
     for ref in (acc_q, acc_k, acc_v, acc_m, acc_g, acc_s, acc_mk, acc_mv):
         ref[...] = jnp.zeros_like(ref)
@@ -202,7 +215,7 @@
         found = jnp.int32(0)
         seen = jnp.int32(0)
         for i in range(requests):
-            ident = ids_s[source, 0, i]
+            ident = ids_s[source, i % picks, i // picks]
             mine = (ident // held) == st
             found = jnp.where(mine & (seen == k), ident % held, found)
             seen = seen + mine.astype(jnp.int32)
@@ -226,28 +239,32 @@
         pass_copy(d).start()
     for k in range(cap):
         landed[st, k] = store[asked(st, k)]
-
-    tok_relay(1)
+    for i in range(3, len(pairs)):
+        loads[i].start()
+
+    for p in range(PIECES):
+        tok_relay(1, p)
 
     for d in range(1, n_st):
         pass_wait(d).wait_recv()
     for i in range(requests):
-        ident = ids_s[st, 0, i]
+        ident = ids_s[st, i % picks, i // picks]
         owner = ident // held
         order = jnp.int32(0)
         for e in range(i):
-            order = order + ((ids_s[st, 0, e] // held) == owner).astype(jnp.int32)
+            order = order + ((ids_s[st, e % picks, e // picks] // held) == owner).astype(jnp.int32)
         rows[me, pl.ds(i * pass_rows, pass_rows), :] = landed[owner, jnp.minimum(order, cap - 1)]
     row_send(None)
 
-    for i in range(2, 9):
+    for i in range(2, len(pairs)):
         loads[i].wait()
 
-    def take_tokens(j):
+    def take_tokens(j, p):
         at = pl.ds(pl.multiple_of(j * cols, cols), cols)
+        step_rows = total // PIECES // SPLIT
 
         def part(c, carry):
-            here = pl.ds(pl.multiple_of(c * 256, 256), 256)
+            here = pl.ds(pl.multiple_of((p * SPLIT + c) * step_rows, step_rows), step_rows)
             x = tok[j, here, :]
             acc_q[here, :] += dot(x, wq[at, :])
             acc_k[here, :] += dot(x, wk[at, :])
@@ -264,17 +281,22 @@
                 squares = squares + slab * slab
             acc_s[here, :] = squares
             return carry
-        lax.fori_loop(0, total // 256, part, 0)
-
-    tok_consume(0, 2, take_tokens)
-
-    def token_stage(d, carry):
-        tok_relay(d)
-        tok_consume(d, d + 1, take_tokens)
-        return carry
-    lax.fori_loop(2, n_z, token_stage, 0)
-
-    row_relay(1)
+        lax.fori_loop(0, SPLIT, part, 0)
+
+    def token_piece(p, carry):
+        tok_consume(0, 2, take_tokens, p)
+        return carry
+    lax.fori_loop(0, PIECES, token_piece, 0)
+
+    def token_stage(q, carry):
+        d, p = q // PIECES, q % PIECES
+        tok_relay(d, p)
+        tok_consume(d, d + 1, take_tokens, p)
+        return carry
+    lax.fori_loop(2 * PIECES, n_z * PIECES, token_stage, 0)
+
+    for p in range(PIECES):
+        row_relay(1, p)
 
     def prepare(c, carry):
         here = pl.ds(pl.multiple_of(c * CHUNK, CHUNK), CHUNK)
@@ -315,24 +337,18 @@
         return carry
     lax.fori_loop(0, total // CHUNK, retain, 0)
 
-    def take_rows(j):
+    def take_rows(j, p):
         at = pl.ds(pl.multiple_of(j * cols, cols), cols)
-
-        def part(c, carry):
-            here = pl.ds(pl.multiple_of(c * 256, 256), 256)
-            x = rows[j, here, :]
-            acc_mk[here, :] += dot(x, wmk[at, :])
-            acc_mv[here, :] += dot(x, wmv[at, :])
-            return carry
-        lax.fori_loop(0, rows.shape[1] // 256, part, 0)
-
-    row_consume(0, 2, take_rows)
-
-    def row_stage(d, carry):
-        row_relay(d)
-        row_consume(d, d + 1, take_rows)
-        return carry
-    lax.fori_loop(2, n_z, row_stage, 0)
+        size = rows.shape[1] // PIECES
+        here = pl.ds(pl.multiple_of(p * size, size), size)
+        x = rows[j, here, :]
+        acc_mk[here, :] += dot(x, wmk[at, :])
+        acc_mv[here, :] += dot(x, wmv[at, :])
+
+    def row_piece(p, carry):
+        row_consume(0, 2, take_rows, p)
+        return carry
+    lax.fori_loop(0, PIECES, row_piece, 0)
 
     blocks = requests // picks
     block = total // blocks
@@ -353,7 +369,17 @@
             lifted = dot(o, lift_ref[h])
             out_ref[here, wide] = (ret[here, wide] + gate[here, h:h + 1] * lifted).astype(BF16)
         return carry
-    lax.fori_loop(0, blocks, attend, 0)
+    def row_stage(q, carry):
+        d, p = q // PIECES, q % PIECES
+        row_relay(d, p)
+        row_consume(d, d + 1, take_rows, p)
+
+        @pl.when(d == n_z - 1)
+        def _():
+            share = blocks // PIECES
+            lax.fori_loop(p * share, (p + 1) * share, attend, 0)
+        return carry
+    lax.fori_loop(2 * PIECES, n_z * PIECES, row_stage, 0)
 
     for d in range(1, n_st):
         id_copy(d).wait_send()
@@ -391,29 +417,30 @@
         key_cols, mem_cols = w_query.shape[1], w_mem_query.shape[1]
         scratch = [
             V((n_tp, total, cols), BF16), V((n_tp, requests * pass_rows, cols), BF16),
+            V(cosine.shape, F32), V(sine.shape, F32), V(w_lift.shape, BF16),
             V(w_query.shape, BF16), V(w_key.shape, BF16), V(w_value.shape, BF16),
             V(w_mem_query.shape, BF16), V(w_mem_key.shape, BF16), V(w_mem_value.shape, BF16),
             V(store.shape, BF16), V((n_st, cap, pass_rows, cols), BF16), V((n_st, cap, pass_rows, cols), BF16),
-            V((n_st, 1, requests), jnp.int32), pltpu.SMEM((n_st, 1, requests), jnp.int32),
+            V((n_st, picks, blocks), jnp.int32), pltpu.SMEM((n_st, picks, blocks), jnp.int32),
             V((total, key_cols), F32), V((total, key_cols), F32), V((total, wide), F32), V((total, mem_cols), F32),
             V((total, heads), F32), V((total, 128), F32),
             V((requests * pass_rows, mem_cols), F32), V((requests * pass_rows, mem_cols), F32),
             V((total, key_cols), BF16), V((total, key_cols), BF16), V((total, wide), BF16), V((total, mem_cols), BF16),
             V((total, wide), F32), V((total, heads), F32),
-            dma((10,)), dma((n_st,)), dma((n_st,)), dma((n_st,)), dma((n_st,)),
-            dma((n_tp,)), dma((n_tp,)), dma((1,)), dma((n_tp,)),
-            dma((n_tp,)), dma((n_tp,)), dma((1,)), dma((n_tp,)),
+            dma((16,)), dma((n_st,)), dma((n_st,)), dma((n_st,)), dma((n_st,)),
+            dma((n_tp, PIECES)), dma((n_tp, PIECES)), dma((1, PIECES)), dma((n_tp, PIECES)),
+            dma((n_tp, PIECES)), dma((n_tp, PIECES)), dma((1, PIECES)), dma((n_tp, PIECES)),
         ]
         return pl.pallas_call(
             functools.partial(kernel, n_st, n_tp, cap, picks, held),
             out_shape=jax.ShapeDtypeStruct((total, heads * VALUE_DIM), BF16),
-            in_specs=[smem] + [hbm] * 7 + [vmem] * 4 + [hbm] * 2,
+            in_specs=[smem] + [hbm] * 7 + [vmem] + [hbm] * 5,
             out_specs=vmem,
             scratch_shapes=scratch,
             compiler_params=pltpu.CompilerParams(
                 collective_id=0, has_side_effects=True, vmem_limit_bytes=60 * 1024 * 1024),
         )(decay_rate, tokens, w_query, w_key, w_value, w_mem_query, w_mem_key, w_mem_value,
-          w_gate.T, w_lift, jnp.asarray(cosine), jnp.asarray(sine), store, passage_ids.reshape(1, requests))
+          w_gate.T, w_lift, jnp.asarray(cosine), jnp.asarray(sine), store, passage_ids.T)
 
     in_specs = (P("st", "tp"),) + (P(None, "tp"),) * 7 + (
         P("tp", None, None), P("tp"), P("st", None, "tp"), P("st", None))

time: 87.1 us -> 82.1 us (0.943)
  Pallas kernels: 83.7 us -> 80 us
  local copies, waits for them, and re-layouts: 3.23 us -> 1.87 us
    pallas_call x1, Pallas kernels: 83.7 us -> 80 us  [per_device(): pl.pallas_call(functools.partial(kernel, n_st, n_tp, cap, picks, held), o...]
    unnamed x2 -> x1, local copies, waits for them, and re-layouts: 2.63 us -> 1.87 us
where the time goes in v1:
time: 82.1 us; the launch traced here: 81.9 us
  Pallas kernels  80 us (97%)
  local copies, waits for them, and re-layouts  1.87 us (2%)
    pallas_call x1, Pallas kernels, per_device(): pl.pallas_call(functools.partial(kernel, n_st, n_tp, cap, picks, held), o...  80 us
    unnamed x1, local copies, waits for them, and re-layouts  1.87 us

profile of v1, /device:TPU:1, one launch (start us, length us, event | category | flops | bytes accessed | tf_op | source)
XLA Modules:
  0.0 81.9 jit_solution(13810576936190177473)
XLA Ops:
  0.0 80.0 %shard_map.136 = bf16[512,512]{1,0:T(8,128)(2,1)} custom-call(f32[2]{0:T(128)} %rate_ref.1, bf16[512,512]{1,0:T(8,128)(2,1)} %tok_hbm.1, bf16[4096,256]{1,0:T(8,128)(2,1)} %wq_hbm.1, bf16[4096,256]{1,0:T(8,128)(2,1)} %wk_hbm.1, bf16[4096,512]{1,0:T(8,128)(2,1)} %wv_hbm.1, bf16[4096,256]{1,0:T(8,128)(2,1)} %wm_hbm.1, bf16[4096,256]{1,0:T(8,128)(2,1)} %wmk_hbm.1, ...), custom_call_target="tpu_custom_call" | custom-call | tf_op jit(solution)/shard_map/pallas_call | solution.py:434
  80.0 1.9 %copy.16 = bf16[512,512]{1,0:T(8,128)(2,1)} copy(bf16[512,512]{1,0:T(8,128)(2,1)} %shard_map.136) | data formatting | bytes 1048576
